TPU v7x, 32 devices: a whole 2x2x4 slice. The times are simulated.
32 devices in a mesh: sp: 8 (over z, x), tp: 4 (over y, core).
Axes of the slice: x: 2, y: 2, z: 4, core: 2. Of those that a mesh axis runs over, the one named last changes fastest.
Arguments:
- tokens: bfloat16 [4096, 2048], P(('sp', 'tp')), may hold values from -6 to 6
- norm_gain: float32 [2048], replicated, may hold values from 0.1 to 1.9
- pool_in_weight: bfloat16 [2048, 1024], P('sp', 'tp'), may hold values from -0.125 to 0.125
- query_weight: bfloat16 [2048, 1024], P('sp', 'tp'), may hold values from -0.125 to 0.125
- forget_weight: bfloat16 [2048, 1024], P('sp', 'tp'), may hold values from -0.125 to 0.125
- input_weight: bfloat16 [2048, 1024], P('sp', 'tp'), may hold values from -0.125 to 0.125
- forget_gap: float32 [1024], P('tp'), may hold values from 0 to 0.02
- decay_shift: float32 [8, 4096], P('tp', 'sp'), may hold values from -0.42 to 0
- out_gain: float32 [128], replicated, may hold values from 0.1 to 1.9
- pool_out_weight: bfloat16 [1024, 2048], P('tp', 'sp'), may hold values from -0.53033009 to 0.53033009
- recur_out_weight: bfloat16 [1024, 2048], P('tp', 'sp'), may hold values from -0.53033009 to 0.53033009
Outputs:
- mixed_out: bfloat16 [4096, 2048], P(('sp', 'tp'))
All inputs are finite; a program needn't handle non-finite values.
Results may differ from a plain program's by a relative error of at most 0.014.
Values may be sent and summed in bfloat16 or wider, within the bound.
A program may use at most 64 MiB of HBM per device.

v0:
```python
import jax
import jax.numpy as jnp
from jax import lax
from jax.sharding import PartitionSpec as P

GROUPS = 4
RDIM = 128
SPAN = 64
EPSILON = 1e-06
EXACT_MATMUL = lax.Precision.HIGHEST


def passed_along(block, axis, distance):
    devices = range(lax.axis_size(axis))
    route = [(i - distance, i) for i in devices if i - distance in devices]
    return lax.ppermute(block, axis, route)


def prefix(part, axis, combine, identity):
    place = lax.axis_index(axis)
    gathered = jax.tree.map(lambda a: lax.all_gather(a, axis), part)
    state = jax.tree.map(lambda a, e: jnp.zeros_like(a) + jnp.asarray(e, a.dtype), part, identity)

    def one(hop, state):
        return combine(
            state, jax.tree.map(lambda a: lax.dynamic_index_in_dim(a, hop, 0, False), gathered)
        )

    return lax.fori_loop(0, place, one, state)


def window_sums(padded, levels, reach):
    length = padded.shape[0] - reach
    results = []
    running = padded
    for level in range(levels):
        width = 2**level
        running = running[width:] + running[:-width]
        offset = reach + 1 - 2 * width
        results.append(lax.slice_in_dim(running, offset, offset + length, axis=0))
    return results


def chain(earlier, later):
    return (earlier[0] * later[0], later[0][:, :, None] * earlier[1] + later[1])


def to_blocks(tensor, block_count, head_count):
    return tensor.reshape(block_count, SPAN, head_count, RDIM).transpose(0, 2, 1, 3)


def local(
    tokens,
    norm_gain,
    pool_in_weight,
    query_weight,
    forget_weight,
    input_weight,
    forget_gap,
    decay_shift,
    out_gain,
    pool_out_weight,
    recur_out_weight,
):
    pool_cols = pool_in_weight.shape[1]
    recur_cols = query_weight.shape[1]
    local_in = jnp.concatenate([pool_in_weight, query_weight, forget_weight, input_weight], axis=1)
    whole_in = lax.all_gather(local_in, "sp", axis=0, tiled=True)
    floats = tokens.astype(jnp.float32)
    scale = lax.rsqrt(jnp.mean(floats * floats, axis=-1, keepdims=True) + EPSILON)
    normed = (floats * scale * norm_gain).astype(jnp.bfloat16)
    pool_weight = whole_in[:, :pool_cols]
    recur_weight = whole_in[:, pool_cols:]
    pooled_in = jnp.dot(
        lax.all_gather(normed, "tp", axis=0, tiled=True),
        pool_weight,
        preferred_element_type=jnp.float32,
    ).astype(jnp.bfloat16)
    recur_in = jnp.dot(
        lax.all_gather(normed, "tp", axis=0, tiled=True),
        recur_weight,
        preferred_element_type=jnp.float32,
    ).astype(jnp.bfloat16)
    query = recur_in[:, :recur_cols].astype(jnp.float32)
    forget_pre = recur_in[:, recur_cols : 2 * recur_cols].astype(jnp.float32)
    values = recur_in[:, 2 * recur_cols :].astype(jnp.float32)
    row_count = pooled_in.shape[0]
    head_count = recur_cols // RDIM
    block_count = row_count // SPAN
    gate_pre = forget_pre.reshape(row_count, head_count, RDIM)
    opened = forget_gap.reshape(head_count, RDIM) * jax.nn.sigmoid(-gate_pre)
    log_decay = jnp.log1p(-opened) + decay_shift.T[:, :, None]
    query_blocks = to_blocks(query, block_count, head_count)
    decay_blocks = to_blocks(log_decay, block_count, head_count)
    key_blocks = to_blocks(opened, block_count, head_count)
    value_blocks = to_blocks(values, block_count, head_count)
    causal = jnp.tril(jnp.ones((SPAN, SPAN), jnp.bool_))
    inner_block_output = jnp.cumsum(decay_blocks, axis=2)
    block_decay_total = inner_block_output[:, :, -1, :]
    decayed_query = query_blocks * jnp.exp(inner_block_output)
    scores = jnp.einsum(
        "bhtk,bhsk->bhts",
        decayed_query,
        key_blocks * jnp.exp(-inner_block_output),
        precision=EXACT_MATMUL,
    )
    scores = jnp.where(causal, scores, 0.0)
    received_output = jnp.einsum("bhts,bhsv->bhtv", scores, value_blocks, precision=EXACT_MATMUL)
    growth_factor = jnp.einsum(
        "bhsk,bhsv->bhkv",
        key_blocks * jnp.exp(block_decay_total[:, :, None, :] - inner_block_output),
        value_blocks,
        precision=EXACT_MATMUL,
    )
    fading = jnp.exp(block_decay_total)

    def carry_step(state_matrix, item):
        return (item[0][:, :, None] * state_matrix + item[1], state_matrix)

    empty_state = jnp.zeros((head_count, RDIM, RDIM), jnp.float32)
    local_state, block_starts = lax.scan(carry_step, empty_state, (fading, growth_factor))
    received_output = received_output + jnp.einsum(
        "bhtk,bhkv->bhtv", decayed_query, block_starts, precision=EXACT_MATMUL
    )
    earlier_total = jnp.cumsum(block_decay_total, axis=0) - block_decay_total
    decay_from_start = query_blocks * jnp.exp(inner_block_output + earlier_total[:, :, None, :])
    device_fade = jnp.exp(jnp.sum(block_decay_total, axis=0))
    reach = 2**GROUPS - 1
    rim = pooled_in[row_count - reach :]
    unit_fade = jnp.ones((head_count, RDIM), jnp.float32)
    previous = passed_along(rim, "sp", 1)
    carried_fade, carried_state = prefix(
        (device_fade, local_state), "sp", chain, (unit_fade, empty_state)
    )
    received_output = received_output + jnp.einsum(
        "fuoy,uyi->fuoi", decay_from_start, carried_state, precision=EXACT_MATMUL
    )
    received_output = received_output.transpose(0, 2, 1, 3).reshape(row_count, head_count, RDIM)
    spread = lax.rsqrt(
        jnp.mean(received_output * received_output, axis=-1, keepdims=True) + EPSILON
    )
    recur_mixed = (
        (received_output * spread * out_gain).astype(jnp.bfloat16).reshape(row_count, recur_cols)
    )
    group = lax.axis_index("tp")
    padded = jnp.concatenate([previous, pooled_in], axis=0).astype(jnp.float32)
    results = window_sums(padded, GROUPS, reach)
    window_sum = results[GROUPS - 1]
    for level in range(GROUPS - 1):
        window_sum = jnp.where(group == level, results[level], window_sum)
    width = jnp.left_shift(jnp.int32(2), group)
    position = lax.axis_index("sp") * row_count + jnp.arange(row_count, dtype=jnp.int32)
    divisor = jnp.minimum(position + 1, width).astype(jnp.float32)[:, None]
    pool_mixed = (window_sum / divisor - pooled_in.astype(jnp.float32)).astype(jnp.bfloat16)
    out_pool, out_recur = (
        lax.all_gather(pool_out_weight, "sp", axis=1, tiled=True),
        lax.all_gather(recur_out_weight, "sp", axis=1, tiled=True),
    )
    partial_value = jnp.dot(pool_mixed, out_pool, preferred_element_type=jnp.float32)
    return lax.psum_scatter(
        (
            partial_value + jnp.dot(recur_mixed, out_recur, preferred_element_type=jnp.float32)
        ).astype(jnp.bfloat16),
        "tp",
        scatter_dimension=0,
        tiled=True,
    )


def solution(mesh):
    in_specs = (
        P(("sp", "tp"), None),
        P(),
        P("sp", "tp"),
        P("sp", "tp"),
        P("sp", "tp"),
        P("sp", "tp"),
        P("tp"),
        P("tp", "sp"),
        P(),
        P("tp", "sp"),
        P("tp", "sp"),
    )
    out_specs = P(("sp", "tp"), None)
    return jax.shard_map(local, mesh=mesh, in_specs=in_specs, out_specs=out_specs, check_vma=False)
```

profile of v0, /device:TPU:0, one launch (start us, length us, event | category | flops | bytes accessed | tf_op | source)
XLA Modules:
  0.0 273.9 jit_solution(6150586459145285040)
XLA Ops:
  6.5 1.3 fusion.7
  7.8 2.0 fusion.9
  9.9 2.0 pad_maximum_fusion
  11.9 0.7 all-gather.13.cloned.1.call-update
  12.9 22.4 %all-gather.9.cloned.1.call-done = bf16[512,2048]{1,0:T(8,128)(2,1)} async-done(((bf16[128,2048]{1,0:T(8,128)(2,1)}), bf16[512,2048]{1,0:T(8,128)(2,1)}) %all-gather.9.cloned.1.call-update) | async-done | bytes 2097168 | tf_op jit(solution)/shard_map/all_gather | solution.py:75
  35.3 74.9 %all-gather.11.cloned.1.call-done = bf16[2048,1024]{1,0:T(8,128)(2,1)} async-done(((bf16[256,1024]{1,0:T(8,128)(2,1)}), bf16[2048,1024]{1,0:T(8,128)(2,1)}) %all-gather.11.cloned.1.call-update) | async-done | bytes 4194320 | tf_op jit(solution)/shard_map/all_gather | solution.py:68
  110.2 4.3 %fusion.2 = bf16[512,768]{1,0:T(8,128)(2,1)S(1)} fusion(bf16[512,2048]{1,0:T(8,128)(2,1)} %all-gather.9.cloned.1.call-done, bf16[2048,1024]{1,0:T(8,128)(2,1)} %all-gather.11.cloned.1.call-done), kind=kOutput, calls=%fused_computation.8 | convolution fusion | flops 1611005952 | bytes 6029312 | tf_op jit(solution)/shard_map/dot_general | solution.py:79
  116.2 1.5 bitcast_multiply_fusion.4
  117.7 1.0 fusion.21
  118.7 6.6 %while.26 = (s32[]{:T(128)}, f32[2,128,128]{2,1,0:T(8,128)S(1)}, f32[8,2,128,128]{3,2,1,0:T(8,128)}, f32[8,2,128]{2,0,1:T(8,128)S(1)}, f32[8,2,128,128]{3,2,1,0:T(8,128)S(1)}, /*index=5*/s32[]{:T(128)}, s32[]{:T(128)}) while((s32[]{:T(128)}, f32[2,128,128]{2,1,0:T(8,128)S(1)}, f32[8,2,128,128]{3,2,1,0:T(8,128)}, ...), condition=%wide.region_3.4_spmd.clone, body=%wide.region_2.3_spmd.clone.sunk | while | flops 131075 | bytes 658540 | solution.py:121
  118.7 0.7 bitcast_dynamic-update-slice_fusion.2
  119.6 0.7 bitcast_dynamic-update-slice_fusion.2
  120.4 0.7 bitcast_dynamic-update-slice_fusion.2
  121.2 0.7 bitcast_dynamic-update-slice_fusion.2
  122.0 0.7 bitcast_dynamic-update-slice_fusion.2
  122.9 0.7 bitcast_dynamic-update-slice_fusion.2
  123.7 0.7 bitcast_dynamic-update-slice_fusion.2
  124.5 0.7 bitcast_dynamic-update-slice_fusion.2
  125.3 0.6 copy-done.1
  126.0 0.5 all-gather.15.cloned.1.call-update
  126.7 2.6 convolution_convert_fusion
  129.3 2.5 collective-permute-start
  131.8 1.2 convolution_select_fusion
  133.4 18.6 %all-gather.2 = f32[8,2,128]{2,1,0:T(2,128)S(1)} all-gather(f32[1,2,128]{2,1,0:T(2,128)S(1)} %exponential_bitcast_fusion), channel_id=2, replica_groups=mesh['sp'=8,'tp'=4] {'sp'}, dimensions={0}, use_global_device_ids=true | all-gather | bytes 9216 | tf_op jit(solution)/shard_map/all_gather | solution.py:21
  152.3 4.1 %fusion.30 = f32[512,2048]{1,0:T(8,128)} fusion(bf16[256,2048]{1,0:T(8,128)(2,1)} %all-gather.13.cloned.1.call-done, bf16[512,256]{1,0:T(8,128)(2,1)S(1)} %convolution_convert_fusion, f32[520,256]{1,0:T(8,128)S(1)} %slice_add_fusion.2, f32[526,256]{1,0:T(8,128)S(1)} %slice_add_fusion.1, f32[524,256]{1,0:T(8,128)S(1)} %slice_add_fusion, ...), kind=kOutput, calls=%fused_computation.54 | convolution fusion | flops 537919488 | bytes 7604227 | tf_op jit(solution)/shard_map/dot_general | solution.py:159
  156.3 35.2 %all-gather.17.cloned.1.call-done = f32[16,128,128]{2,1,0:T(8,128)} async-done(((f32[2,128,128]{2,1,0:T(8,128)}), f32[16,128,128]{2,1,0:T(8,128)}) %all-gather.17.cloned.1.call-update) | async-done | bytes 1048592 | tf_op jit(solution)/shard_map/all_gather | solution.py:21
  191.7 0.7 convolution_bitcast_fusion
  192.4 2.6 multiply_reduce_fusion
  195.6 36.0 %all-gather.15.cloned.1.call-done = bf16[256,2048]{1,0:T(8,128)(2,1)} async-done(((bf16[256,256]{1,0:T(8,128)(2,1)}), bf16[256,2048]{1,0:T(8,128)(2,1)}) %all-gather.15.cloned.1.call-update) | async-done | bytes 1048592 | tf_op jit(solution)/shard_map/all_gather | solution.py:157
  231.5 0.6 mul.113
  232.1 4.6 %add_convert_fusion = bf16[512,2048]{1,0:T(8,128)(2,1)} fusion(f32[512,2048]{1,0:T(8,128)} %fusion.30, bf16[256,2048]{1,0:T(8,128)(2,1)} %all-gather.15.cloned.1.call-done, f32[64,8,2,128]{3,2,1,0:T(2,128)S(1)} %bitcast.79, f32[64,8,2,128]{3,2,1,0:T(2,128)S(1)} %bitcast.78, f32[256]{0:T(256)S(1)} %broadcast_bitcast_fusion), kind=kOutput, calls=%fused_computation.5 | convolution fusion | flops 539361280 | bytes 8389632 | tf_op jit(solution)/shard_map/dot_general | solution.py:162
  236.7 30.3 %reduce-scatter.2.cloned.1.call-done = bf16[128,2048]{1,0:T(8,128)(2,1)} async-done(((bf16[512,2048]{1,0:T(8,128)(2,1)}), bf16[128,2048]{1,0:T(8,128)(2,1)}) %reduce-scatter.2.cloned.1.call-update) | async-done | bytes 524304 | tf_op jit(solution)/shard_map/reduce_scatter | solution.py:160
  (67 shorter events, 4.4 us)
Async XLA Ops:
  6.5 120.1 %copy-start = (f32[128]{0:T(128)S(1)}, f32[128]{0:T(128)}, u32[]{:S(2)}) copy-start(f32[128]{0:T(128)} %param.23) | copy-start | bytes 1540
  6.5 6.2 %copy-start.3 = (f32[2,512]{1,0:T(2,128)S(1)}, f32[2,512]{1,0:T(2,128)}, u32[]{:S(2)}) copy-start(f32[2,512]{1,0:T(2,128)} %param.22) | copy-start | bytes 12292
  6.5 28.8 %all-gather.9.cloned.1.call-start = ((), (), s32[]{:S(2)}) async-start(), calls=%async_computation.1 | async-start | bytes 2621440 | tf_op jit(solution)/shard_map/all_gather | solution.py:75
  9.9 100.4 %all-gather.11.cloned.1.call-start = ((), (), s32[]{:S(2)}) async-start(), calls=%async_computation.2 | async-start | bytes 4718592 | tf_op jit(solution)/shard_map/all_gather | solution.py:68
  11.9 140.4 %all-gather.13.cloned.1.call-start = ((), (), s32[]{:S(2)}) async-start(), calls=%async_computation.3 | async-start | bytes 1179648 | tf_op jit(solution)/shard_map/all_gather | solution.py:156
  12.6 178.9 %all-gather.17.cloned.1.call-start = ((), (), s32[]{:S(2)}) async-start(), calls=%async_computation.6 | async-start | bytes 1179648 | tf_op jit(solution)/shard_map/all_gather | solution.py:21
  114.6 0.7 copy-start.4
  125.3 0.7 copy-start.1
  126.0 105.5 %all-gather.15.cloned.1.call-start = ((), (), s32[]{:S(2)}) async-start(), calls=%async_computation.4 | async-start | bytes 1179648 | tf_op jit(solution)/shard_map/all_gather | solution.py:157
  126.6 140.5 %reduce-scatter.2.cloned.1.call-start = ((), (), s32[]{:S(2)}) async-start(), calls=%async_computation.5 | async-start | bytes 2621440 | tf_op jit(solution)/shard_map/reduce_scatter | solution.py:160
  129.3 22.7 %collective-permute-start = (bf16[15,256]{1,0:T(8,128)(2,1)S(1)}, bf16[15,256]{1,0:T(8,128)(2,1)S(1)}, u32[]{:S(2)}, u32[]{:S(2)}) collective-permute-start(bf16[15,256]{1,0:T(8,128)(2,1)S(1)} %slice.70), channel_id=1, source_target_pairs={{0,4},{4,8},{8,12},{12,16},{16,20},{20,24},{24,28},{1,5},{5,9},{9,... | collective-permute-start | bytes 23048 | tf_op jit(solution)/shard_map/ppermute | solution.py:16
  152.2 39.5 %copy-start.2 = (f32[8,2,64,128]{3,0,1,2:T(8,128)S(1)}, f32[8,2,64,128]{3,0,1,2:T(8,128)}, u32[]{:S(2)}) copy-start(f32[8,2,64,128]{3,0,1,2:T(8,128)} %get-tuple-element.146) | copy-start | bytes 1572868
Sparse Core Ops, SparseCore 0:
  10.0 25.2 all-gather.8
  37.4 72.7 all-gather.10
  112.3 37.9 all-gather.12
  152.2 39.1 all-gather.16
  193.4 38.0 all-gather.14
  236.8 30.1 reduce-scatter.1
where the time goes:
time: 274 us
  waiting for transfers between devices  200 us (73%)
  matrix products  21.4 us (8%)
  blocking collectives  18.6 us (7%)
  other arithmetic  14 us (5%)
  between operations  13.8 us (5%)
  local copies, waits for them, and re-layouts  2.88 us (1%)
    all_gather x1, waiting for transfers between devices, local(): whole_in = lax.all_gather(local_in, 'sp', axis=0, tiled=True)  74.9 us
    all_gather x1, waiting for transfers between devices, local(): lax.all_gather(recur_out_weight, 'sp', axis=1, tiled=True)  36 us
    all_gather x1, waiting for transfers between devices, prefix(): gathered = jax.tree.map(lambda a: lax.all_gather(a, axis), part)  35.2 us
    reduce_scatter x1, waiting for transfers between devices, local(): lax.psum_scatter((partial_value + jnp.dot(recur_mixed, out_recur, preferr...  30.3 us
    all_gather x1, waiting for transfers between devices, local(): lax.all_gather(normed, 'tp', axis=0, tiled=True)  22.4 us
    all_gather x1, blocking collectives, prefix(): gathered = jax.tree.map(lambda a: lax.all_gather(a, axis), part)  18.6 us
  transfers between devices with their start and end apart: 7, of which 5 were waited for; matrix products, arithmetic and copies ran while one was open for 11% of the time, Pallas kernels for 0%

commit v1 on v0

--- a/solution.py
+++ b/solution.py
@@ -65,7 +65,12 @@
     pool_cols = pool_in_weight.shape[1]
     recur_cols = query_weight.shape[1]
     local_in = jnp.concatenate([pool_in_weight, query_weight, forget_weight, input_weight], axis=1)
-    whole_in = lax.all_gather(local_in, "sp", axis=0, tiled=True)
+    ring = [local_in]
+    for hop_ in range(7):
+        ring.append(lax.ppermute(ring[-1], "sp", [(dev, (dev + 1) % 8) for dev in range(8)]))
+    whole_in = jnp.roll(
+        jnp.concatenate(ring[::-1], axis=0), (lax.axis_index("sp") + 1) * ring[0].shape[0], axis=0
+    )
     floats = tokens.astype(jnp.float32)
     scale = lax.rsqrt(jnp.mean(floats * floats, axis=-1, keepdims=True) + EPSILON)
     normed = (floats * scale * norm_gain).astype(jnp.bfloat16)

time: 274 us -> 264 us (0.964)
  waiting for transfers between devices: 200 us -> 169 us
  local copies, waits for them, and re-layouts: 2.88 us -> 25 us
    ppermute x0 -> x7, waiting for transfers between devices: none -> 92.4 us  [local(): lax.ppermute(ring[-1], 'sp', [(dev, (dev + 1) % 8) for dev in range(8)])]
    all_gather x1 -> x0, waiting for transfers between devices: 74.9 us -> none  [local(): whole_in = lax.all_gather(local_in, 'sp', axis=0, tiled=True)]
    all_gather x1, waiting for transfers between devices: 35.2 us -> 9.69 us  [prefix(): gathered = jax.tree.map(lambda a: lax.all_gather(a, axis), part)]
    all_gather x1, waiting for transfers between devices: 22.4 us -> 0.01 us  [local(): lax.all_gather(normed, 'tp', axis=0, tiled=True)]
    unnamed x11 -> x40, local copies, waits for them, and re-layouts: 0.84 us -> 21 us
    ppermute x0 -> x7, starting transfers between devices: none -> 3.04 us  [local(): lax.ppermute(ring[-1], 'sp', [(dev, (dev + 1) % 8) for dev in range(8)])]
  transfers between devices with their start and end apart: 7 -> 13, of which waited for: 5 -> 10; matrix products, arithmetic and copies ran while one was open for 11% -> 20% of each run, Pallas kernels for 0% -> 0%
where the time goes in v1:
time: 264 us
  waiting for transfers between devices  169 us (64%)
  local copies, waits for them, and re-layouts  25 us (9%)
  matrix products  21.4 us (8%)
  blocking collectives  16.3 us (6%)
  between operations  13.5 us (5%)
  other arithmetic  13.3 us (5%)
  starting transfers between devices  4.62 us (2%)
    ppermute x7, waiting for transfers between devices, local(): lax.ppermute(ring[-1], 'sp', [(dev, (dev + 1) % 8) for dev in range(8)])  92.4 us
    all_gather x1, waiting for transfers between devices, local(): lax.all_gather(recur_out_weight, 'sp', axis=1, tiled=True)  36 us
    reduce_scatter x1, waiting for transfers between devices, local(): lax.psum_scatter((partial_value + jnp.dot(recur_mixed, out_recur, preferr...  30.3 us
    unnamed x40, local copies, waits for them, and re-layouts  21 us
    all_gather x1, blocking collectives, prefix(): gathered = jax.tree.map(lambda a: lax.all_gather(a, axis), part)  16.3 us
    all_gather x1, waiting for transfers between devices, prefix(): gathered = jax.tree.map(lambda a: lax.all_gather(a, axis), part)  9.69 us
    dynamic_update_slice x8, other arithmetic, local(): lax.scan(carry_step, empty_state, (fading, growth_factor))  5.34 us
  transfers between devices with their start and end apart: 13, of which 10 were waited for; matrix products, arithmetic and copies ran while one was open for 20% of the time, Pallas kernels for 0%

profile of v1, /device:TPU:0, one launch (start us, length us, event | category | flops | bytes accessed | tf_op | source)
XLA Modules:
  0.0 263.6 jit_solution(16939507877176380439)
XLA Ops:
  6.5 1.2 pad_maximum_fusion
  7.8 3.0 %collective-permute-start = (bf16[256,1024]{1,0:T(8,128)(2,1)S(1)}, bf16[256,1024]{1,0:T(8,128)(2,1)S(1)}, u32[]{:S(2)}, u32[]{:S(2)}) collective-permute-start(bf16[256,1024]{1,0:T(8,128)(2,1)S(1)} %pad_maximum_fusion), channel_id=1, source_target_pairs={{0,4},{4,8},{8,12},{12,16},{16,20},{20,24},{24,28},{28,0},{1,5},{5... | collective-permute-start | bytes 1572872 | tf_op jit(solution)/shard_map/ppermute | solution.py:70
  10.8 1.2 fusion.7
  12.0 2.0 fusion.9
  14.1 11.6 %collective-permute-done = bf16[256,1024]{1,0:T(8,128)(2,1)S(1)} collective-permute-done((bf16[256,1024]{1,0:T(8,128)(2,1)S(1)}, bf16[256,1024]{1,0:T(8,128)(2,1)S(1)}, u32[]{:S(2)}, u32[]{:S(2)}) %collective-permute-start) | collective-permute-done | bytes 524320 | tf_op jit(solution)/shard_map/ppermute | solution.py:70
  25.7 15.8 %collective-permute-done.1 = bf16[256,1024]{1,0:T(8,128)(2,1)S(1)} collective-permute-done((bf16[256,1024]{1,0:T(8,128)(2,1)S(1)}, bf16[256,1024]{1,0:T(8,128)(2,1)S(1)}, u32[]{:S(2)}, u32[]{:S(2)}) %collective-permute-start.1) | collective-permute-done | bytes 524320 | tf_op jit(solution)/shard_map/ppermute | solution.py:70
  41.5 14.9 %collective-permute-done.2 = bf16[256,1024]{1,0:T(8,128)(2,1)S(1)} collective-permute-done((bf16[256,1024]{1,0:T(8,128)(2,1)S(1)}, bf16[256,1024]{1,0:T(8,128)(2,1)S(1)}, u32[]{:S(2)}, u32[]{:S(2)}) %collective-permute-start.2) | collective-permute-done | bytes 524320 | tf_op jit(solution)/shard_map/ppermute | solution.py:70
  56.5 14.1 %collective-permute-done.3 = bf16[256,1024]{1,0:T(8,128)(2,1)S(1)} collective-permute-done((bf16[256,1024]{1,0:T(8,128)(2,1)S(1)}, bf16[256,1024]{1,0:T(8,128)(2,1)S(1)}, u32[]{:S(2)}, u32[]{:S(2)}) %collective-permute-start.3) | collective-permute-done | bytes 524320 | tf_op jit(solution)/shard_map/ppermute | solution.py:70
  70.5 13.2 %collective-permute-done.4 = bf16[256,1024]{1,0:T(8,128)(2,1)S(1)} collective-permute-done((bf16[256,1024]{1,0:T(8,128)(2,1)S(1)}, bf16[256,1024]{1,0:T(8,128)(2,1)S(1)}, u32[]{:S(2)}, u32[]{:S(2)}) %collective-permute-start.4) | collective-permute-done | bytes 524320 | tf_op jit(solution)/shard_map/ppermute | solution.py:70
  83.8 12.4 %collective-permute-done.5 = bf16[256,1024]{1,0:T(8,128)(2,1)S(1)} collective-permute-done((bf16[256,1024]{1,0:T(8,128)(2,1)S(1)}, bf16[256,1024]{1,0:T(8,128)(2,1)S(1)}, u32[]{:S(2)}, u32[]{:S(2)}) %collective-permute-start.5) | collective-permute-done | bytes 524320 | tf_op jit(solution)/shard_map/ppermute | solution.py:70
  97.7 10.4 %collective-permute-done.6 = bf16[256,1024]{1,0:T(8,128)(2,1)} collective-permute-done((bf16[256,1024]{1,0:T(8,128)(2,1)S(1)}, bf16[256,1024]{1,0:T(8,128)(2,1)}, u32[]{:S(2)}, u32[]{:S(2)}) %collective-permute-start.6) | collective-permute-done | bytes 524320 | tf_op jit(solution)/shard_map/ppermute | solution.py:70
  108.2 1.9 constant_dynamic-update-slice_fusion.15
  110.9 0.8 constant_dynamic-update-slice_fusion.13
  111.7 0.9 constant_dynamic-update-slice_fusion.12
  116.4 1.6 constant_dynamic-update-slice_fusion.20
  118.0 1.6 constant_dynamic-update-slice_fusion.19
  119.6 1.9 constant_dynamic-update-slice_fusion.7
  122.3 0.8 constant_dynamic-update-slice_fusion.5
  129.2 4.3 %fusion.2 = bf16[512,768]{1,0:T(8,128)(2,1)S(1)} fusion(bf16[512,2048]{1,0:T(8,128)(2,1)} %all-gather.8.cloned.1.call-done, bf16[4096,1024]{1,0:T(8,128)(2,1)} %constant_dynamic-update-slice_fusion.16, s32[]{:T(128)S(6)} %select_n.48, s32[]{:T(128)S(6)} %add.160), kind=kOutput, calls=%fused_computation.8 | convolution fusion | flops 1611005952 | bytes 6029320 | tf_op jit(solution)/shard_map/dot_general | solution.py:84
  135.0 1.5 bitcast_multiply_fusion.4
  136.5 1.0 fusion.21
  137.5 6.5 %while.26 = (s32[]{:T(128)}, f32[2,128,128]{2,1,0:T(8,128)S(1)}, f32[8,2,128,128]{3,2,1,0:T(8,128)}, f32[8,2,128]{2,0,1:T(8,128)S(1)}, f32[8,2,128,128]{3,2,1,0:T(8,128)S(1)}, /*index=5*/s32[]{:T(128)}, s32[]{:T(128)}) while((s32[]{:T(128)}, f32[2,128,128]{2,1,0:T(8,128)S(1)}, f32[8,2,128,128]{3,2,1,0:T(8,128)}, ...), condition=%wide.region_3.4_spmd.clone, body=%wide.region_2.3_spmd.clone.sunk | while | flops 131075 | bytes 659040 | solution.py:126
  145.5 1.2 convolution_select_fusion
  147.1 2.6 convolution_convert_fusion
  149.7 1.4 collective-permute-start.7
  151.2 16.3 %all-gather.2 = f32[8,2,128]{2,1,0:T(2,128)S(1)} all-gather(f32[1,2,128]{2,1,0:T(2,128)S(1)} %exponential_bitcast_fusion), channel_id=2, replica_groups=mesh['sp'=8,'tp'=4] {'sp'}, dimensions={0}, use_global_device_ids=true | all-gather | bytes 9216 | tf_op jit(solution)/shard_map/all_gather | solution.py:21
  167.8 4.0 %fusion.30 = f32[512,2048]{1,0:T(8,128)} fusion(bf16[256,2048]{1,0:T(8,128)(2,1)} %all-gather.10.cloned.1.call-done, bf16[512,256]{1,0:T(8,128)(2,1)S(1)} %convolution_convert_fusion, f32[520,256]{1,0:T(8,128)S(1)} %slice_add_fusion.2, f32[526,256]{1,0:T(8,128)S(1)} %slice_add_fusion.1, f32[524,256]{1,0:T(8,128)S(1)} %slice_add_fusion, ...), kind=kOutput, calls=%fused_computation.54 | convolution fusion | flops 537919488 | bytes 7604227 | tf_op jit(solution)/shard_map/dot_general | solution.py:164
  171.8 9.7 %all-gather.14.cloned.1.call-done = f32[16,128,128]{2,1,0:T(8,128)} async-done(((f32[2,128,128]{2,1,0:T(8,128)}), f32[16,128,128]{2,1,0:T(8,128)}) %all-gather.14.cloned.1.call-update) | async-done | bytes 1048592 | tf_op jit(solution)/shard_map/all_gather | solution.py:21
  182.4 2.6 multiply_reduce_fusion
  185.5 36.0 %all-gather.12.cloned.1.call-done = bf16[256,2048]{1,0:T(8,128)(2,1)} async-done(((bf16[256,256]{1,0:T(8,128)(2,1)}), bf16[256,2048]{1,0:T(8,128)(2,1)}) %all-gather.12.cloned.1.call-update) | async-done | bytes 1048592 | tf_op jit(solution)/shard_map/all_gather | solution.py:162
  222.1 4.6 %add_convert_fusion = bf16[512,2048]{1,0:T(8,128)(2,1)} fusion(f32[512,2048]{1,0:T(8,128)} %fusion.30, bf16[256,2048]{1,0:T(8,128)(2,1)} %all-gather.12.cloned.1.call-done, f32[64,8,2,128]{3,2,1,0:T(2,128)S(1)} %bitcast.79, f32[64,8,2,128]{3,2,1,0:T(2,128)S(1)} %bitcast.78, f32[256]{0:T(256)S(1)} %broadcast_bitcast_fusion), kind=kOutput, calls=%fused_computation.5 | convolution fusion | flops 539361280 | bytes 8389632 | tf_op jit(solution)/shard_map/dot_general | solution.py:167
  226.7 30.3 %reduce-scatter.2.cloned.1.call-done = bf16[128,2048]{1,0:T(8,128)(2,1)} async-done(((bf16[512,2048]{1,0:T(8,128)(2,1)}), bf16[128,2048]{1,0:T(8,128)(2,1)}) %reduce-scatter.2.cloned.1.call-update) | async-done | bytes 524304 | tf_op jit(solution)/shard_map/reduce_scatter | solution.py:165
  (108 shorter events, 25.0 us)
Async XLA Ops:
  6.5 138.9 %copy-start = (f32[128]{0:T(128)S(1)}, f32[128]{0:T(128)}, u32[]{:S(2)}) copy-start(f32[128]{0:T(128)} %param.23) | copy-start | bytes 1540
  6.5 108.5 %copy-start.3 = (bf16[256,256]{1,0:T(8,128)(2,1)S(1)}, bf16[256,256]{1,0:T(8,128)(2,1)}, u32[]{:S(2)}) copy-start(bf16[256,256]{1,0:T(8,128)(2,1)} %param.17) | copy-start | bytes 393220
  6.5 109.2 %copy-start.4 = (bf16[256,256]{1,0:T(8,128)(2,1)S(1)}, bf16[256,256]{1,0:T(8,128)(2,1)}, u32[]{:S(2)}) copy-start(bf16[256,256]{1,0:T(8,128)(2,1)} %param.18) | copy-start | bytes 393220
  6.5 122.7 %all-gather.8.cloned.1.call-start = ((), (), s32[]{:S(2)}) async-start(), calls=%async_computation.1 | async-start | bytes 2621440 | tf_op jit(solution)/shard_map/all_gather | solution.py:80
  7.8 18.0 %collective-permute-start = (bf16[256,1024]{1,0:T(8,128)(2,1)S(1)}, bf16[256,1024]{1,0:T(8,128)(2,1)S(1)}, u32[]{:S(2)}, u32[]{:S(2)}) collective-permute-start(bf16[256,1024]{1,0:T(8,128)(2,1)S(1)} %pad_maximum_fusion), channel_id=1, source_target_pairs={{0,4},{4,8},{8,12},{12,16},{16,20},{20,24},{24,28},{28,0},{1,5},{5... | collective-permute-start | bytes 1572872 | tf_op jit(solution)/shard_map/ppermute | solution.py:70
  14.1 153.7 %all-gather.10.cloned.1.call-start = ((), (), s32[]{:S(2)}) async-start(), calls=%async_computation.2 | async-start | bytes 1179648 | tf_op jit(solution)/shard_map/all_gather | solution.py:161
  25.7 15.8 %collective-permute-start.1 = (bf16[256,1024]{1,0:T(8,128)(2,1)S(1)}, bf16[256,1024]{1,0:T(8,128)(2,1)S(1)}, u32[]{:S(2)}, u32[]{:S(2)}) collective-permute-start(bf16[256,1024]{1,0:T(8,128)(2,1)S(1)} %collective-permute-done), channel_id=1, source_target_pairs={{0,4},{4,8},{8,12},{12,16},{16,20},{20,24},{24,28},{28,0},{1,5},{5... | collective-permute-start | bytes 1572872 | tf_op jit(solution)/shard_map/ppermute | solution.py:70
  41.5 14.9 %collective-permute-start.2 = (bf16[256,1024]{1,0:T(8,128)(2,1)S(1)}, bf16[256,1024]{1,0:T(8,128)(2,1)S(1)}, u32[]{:S(2)}, u32[]{:S(2)}) collective-permute-start(bf16[256,1024]{1,0:T(8,128)(2,1)S(1)} %collective-permute-done.1), channel_id=1, source_target_pairs={{0,4},{4,8},{8,12},{12,16},{16,20},{20,24},{24,28},{28,0},{1,5},{5... | collective-permute-start | bytes 1572872 | tf_op jit(solution)/shard_map/ppermute | solution.py:70
  56.5 14.1 %collective-permute-start.3 = (bf16[256,1024]{1,0:T(8,128)(2,1)S(1)}, bf16[256,1024]{1,0:T(8,128)(2,1)S(1)}, u32[]{:S(2)}, u32[]{:S(2)}) collective-permute-start(bf16[256,1024]{1,0:T(8,128)(2,1)S(1)} %collective-permute-done.2), channel_id=1, source_target_pairs={{0,4},{4,8},{8,12},{12,16},{16,20},{20,24},{24,28},{28,0},{1,5},{5... | collective-permute-start | bytes 1572872 | tf_op jit(solution)/shard_map/ppermute | solution.py:70
  70.5 13.2 %collective-permute-start.4 = (bf16[256,1024]{1,0:T(8,128)(2,1)S(1)}, bf16[256,1024]{1,0:T(8,128)(2,1)S(1)}, u32[]{:S(2)}, u32[]{:S(2)}) collective-permute-start(bf16[256,1024]{1,0:T(8,128)(2,1)S(1)} %collective-permute-done.3), channel_id=1, source_target_pairs={{0,4},{4,8},{8,12},{12,16},{16,20},{20,24},{24,28},{28,0},{1,5},{5... | collective-permute-start | bytes 1572872 | tf_op jit(solution)/shard_map/ppermute | solution.py:70
  83.7 12.4 %collective-permute-start.5 = (bf16[256,1024]{1,0:T(8,128)(2,1)S(1)}, bf16[256,1024]{1,0:T(8,128)(2,1)S(1)}, u32[]{:S(2)}, u32[]{:S(2)}) collective-permute-start(bf16[256,1024]{1,0:T(8,128)(2,1)S(1)} %collective-permute-done.4), channel_id=1, source_target_pairs={{0,4},{4,8},{8,12},{12,16},{16,20},{20,24},{24,28},{28,0},{1,5},{5... | collective-permute-start | bytes 1572872 | tf_op jit(solution)/shard_map/ppermute | solution.py:70
  96.1 12.1 %collective-permute-start.6 = (bf16[256,1024]{1,0:T(8,128)(2,1)S(1)}, bf16[256,1024]{1,0:T(8,128)(2,1)}, u32[]{:S(2)}, u32[]{:S(2)}) collective-permute-start(bf16[256,1024]{1,0:T(8,128)(2,1)S(1)} %collective-permute-done.5), channel_id=1, source_target_pairs={{0,4},{4,8},{8,12},{12,16},{16,20},{20,24},{24,28},{28,0},{1,5},{5... | collective-permute-start | bytes 1572872 | tf_op jit(solution)/shard_map/ppermute | solution.py:70
  96.1 85.3 %all-gather.14.cloned.1.call-start = ((), (), s32[]{:S(2)}) async-start(), calls=%async_computation.5 | async-start | bytes 1179648 | tf_op jit(solution)/shard_map/all_gather | solution.py:21
  97.7 30.1 %copy-start.5 = (bf16[256,256]{1,0:T(8,128)(2,1)S(1)}, bf16[256,256]{1,0:T(8,128)(2,1)}, u32[]{:S(2)}) copy-start(bf16[256,256]{1,0:T(8,128)(2,1)} %param.19) | copy-start | bytes 393220
  97.7 30.8 %copy-start.6 = (bf16[256,256]{1,0:T(8,128)(2,1)S(1)}, bf16[256,256]{1,0:T(8,128)(2,1)}, u32[]{:S(2)}) copy-start(bf16[256,256]{1,0:T(8,128)(2,1)} %param.20) | copy-start | bytes 393220
  125.6 8.4 %copy-start.7 = (f32[8,64,2]{0,2,1:T(2,128)S(1)}, f32[8,64,2]{0,2,1:T(2,128)}, u32[]{:S(2)}) copy-start(f32[8,64,2]{0,2,1:T(2,128)} %copy.57) | copy-start | bytes 12292
  125.6 8.4 %copy-start.8 = (f32[256]{0:T(256)S(1)}, f32[256]{0:T(256)}, u32[]{:S(2)}) copy-start(f32[256]{0:T(256)} %param.21) | copy-start | bytes 3076
  144.1 0.7 copy-start.1
  144.8 76.7 %all-gather.12.cloned.1.call-start = ((), (), s32[]{:S(2)}) async-start(), calls=%async_computation.3 | async-start | bytes 1179648 | tf_op jit(solution)/shard_map/all_gather | solution.py:162
  145.4 111.7 %reduce-scatter.2.cloned.1.call-start = ((), (), s32[]{:S(2)}) async-start(), calls=%async_computation.4 | async-start | bytes 2621440 | tf_op jit(solution)/shard_map/reduce_scatter | solution.py:165
  149.7 32.0 %copy-start.2 = (f32[8,2,64,128]{3,0,1,2:T(8,128)S(1)}, f32[8,2,64,128]{3,0,1,2:T(8,128)}, u32[]{:S(2)}) copy-start(f32[8,2,64,128]{3,0,1,2:T(8,128)} %get-tuple-element.146) | copy-start | bytes 1572868
  149.7 17.7 %collective-permute-start.7 = (bf16[15,256]{1,0:T(8,128)(2,1)S(1)}, bf16[15,256]{1,0:T(8,128)(2,1)S(1)}, u32[]{:S(2)}, u32[]{:S(2)}) collective-permute-start(bf16[15,256]{1,0:T(8,128)(2,1)S(1)} %slice.69), channel_id=1, source_target_pairs={{0,4},{4,8},{8,12},{12,16},{16,20},{20,24},{24,28},{1,5},{5,9},{9,... | collective-permute-start | bytes 23048 | tf_op jit(solution)/shard_map/ppermute | solution.py:16
Sparse Core Ops, SparseCore 0:
  14.2 22.8 all-gather.7
  96.3 39.8 all-gather.9
  144.9 36.5 all-gather.13
  183.4 38.0 all-gather.11
  226.9 30.1 reduce-scatter.1
